TPU v7x, 32 devices: a whole 2x2x4 slice. The times are simulated.
32 devices in a mesh: fs: 4 (over y, x), tp: 8 (over z, core).
Axes of the slice: x: 2, y: 2, z: 4, core: 2. Of those that a mesh axis runs over, the one named last changes fastest.
Arguments:
- inputs: bfloat16 [8, 320, 2048], P('tp'), may hold values from -6 to 6
- cotangent: bfloat16 [8, 320, 2048], P('tp'), may hold values from -8 to 8
- gate_weight: bfloat16 [2048, 5632], P('tp', 'fs'), may hold values from -0.125 to 0.125
- up_weight: bfloat16 [2048, 5632], P('tp', 'fs'), may hold values from -0.125 to 0.125
- down_weight: bfloat16 [5632, 2048], P('fs', 'tp'), may hold values from -0.078125 to 0.078125
Outputs:
- input_grad: bfloat16 [8, 320, 2048], P('tp')
- down_grad: float32 [5632, 2048], P('fs', 'tp')
All inputs are finite; a program needn't handle non-finite values.
Results may differ from a plain program's by a relative error of at most 0.023.
Values may be sent and summed in bfloat16 or wider, within the bound.
A program may use at most 64 MiB of HBM per device.

v0:
```python
import functools

import jax
import jax.numpy as jnp
from jax import lax
from jax.experimental import pallas as pl
from jax.experimental.pallas import tpu as pltpu
from jax.sharding import PartitionSpec as P

MESH = pl.DeviceIdType.MESH
BF16 = jnp.bfloat16
F32 = jnp.float32


def contract_hidden(left, right):
    return lax.dot_general(left, right, (((1,), (1,)), ((), ())), preferred_element_type=F32)


def contract_tokens(left, right):
    return lax.dot_general(left, right, (((0,), (0,)), ((), ())), preferred_element_type=F32)


def gathered(inputs, cotangent, gate_weight, up_weight, down_weight):
    rows_in = inputs[0]
    rows_grad = cotangent[0]
    token_count, model_width = rows_in.shape
    gate_full = lax.all_gather(gate_weight, "tp", axis=0, tiled=True)
    up_full = lax.all_gather(up_weight, "tp", axis=0, tiled=True)
    down_tall = lax.all_gather(down_weight.T, "tp", axis=0, tiled=True)
    gate_pre = jnp.dot(rows_in, gate_full, preferred_element_type=F32)
    up_pre = jnp.dot(rows_in, up_full, preferred_element_type=F32)
    sig = jax.nn.sigmoid(gate_pre)
    hidden = (gate_pre * sig * up_pre).astype(BF16)
    hidden_grad = jnp.dot(rows_grad, down_tall, preferred_element_type=F32)
    gate_grad = (hidden_grad * up_pre * sig * (1.0 + gate_pre * (1.0 - sig))).astype(BF16)
    up_grad = (hidden_grad * gate_pre * sig).astype(BF16)
    partial_down = contract_tokens(hidden, rows_grad)
    down_grad = lax.psum_scatter(
        partial_down.astype(BF16), "tp", scatter_dimension=1, tiled=True
    ).astype(F32)
    own_sum = lax.psum_scatter(
        (contract_hidden(gate_grad, gate_full) + contract_hidden(up_grad, up_full)).astype(BF16),
        "fs",
        scatter_dimension=0,
        tiled=True,
    )
    whole_grad = lax.all_gather(own_sum, "fs", axis=0, tiled=True)
    return (whole_grad.reshape(1, token_count, model_width), down_grad)


def kernel(
    n_tp, x_ref, ct_ref, wg_ref, wu_ref, wd_ref, grad_ref, down_ref,
    tok, part, core_in, half_in, quarter_in, chain_in, wts, acc, down_out, down_in,
    gate_t, up_t, loc_sem, tok_rs, z_ss, xy_ss, dg_ss, d2d_ss, d2d_rs, w_ss, w_rs, core_ss, core_rs,
    half_ss, half_rs, q_ss, q_rs, ch_ss, ch_rs, ag_ss, ag_rs, dn_ss, dn_rs,
):
    f, t = lax.axis_index("fs"), lax.axis_index("tp")
    n_z = n_tp // 2
    z, c = t // 2, t % 2
    fy, fx = f // 2, f % 2
    f_x = fy * 2 + (1 - fx)
    f_y = (1 - fy) * 2 + fx
    f_d = (1 - fy) * 2 + (1 - fx)
    dev_x, dev_y, dev_d = {"fs": f_x}, {"fs": f_y}, {"fs": f_d}
    partner = {"tp": z * 2 + (1 - c)}
    n_tok, width = tok.shape[2], tok.shape[3]
    qr = n_tok // 4
    hid = wts.shape[1]
    cols = width // n_tp

    def plane(delta):
        return {"tp": (z + delta) * 2 + c}

    def rc(src, dst, ss, rs, dev):
        return pltpu.make_async_remote_copy(
            src_ref=src, dst_ref=dst, send_sem=ss, recv_sem=rs, device_id=dev, device_id_type=MESH
        )

    def qs(q):
        return pl.ds(pl.multiple_of(q * qr, qr), qr)

    def tokq(arr, span, q):
        return tok.at[arr, span, qs(q)]

    own = [
        pltpu.make_async_copy(x_ref.at[0], tok.at[0, t], loc_sem.at[0]),
        pltpu.make_async_copy(ct_ref.at[0], tok.at[1, t], loc_sem.at[1]),
    ]
    own_cols = pl.ds(pl.multiple_of(t * cols, cols), cols)
    for copy in own:
        copy.start()

    barrier = pltpu.get_barrier_semaphore()
    for dev in (dev_x, dev_y, dev_d):
        pl.semaphore_signal(barrier, inc=1, device_id=dev, device_id_type=MESH)
    for k in range(1, n_tp):
        pl.semaphore_signal(barrier, inc=1, device_id={"tp": (t + k) % n_tp}, device_id_type=MESH)
    pl.semaphore_wait(barrier, 3 + n_tp - 1)
    for copy in own:
        copy.wait()

    def z_copy(arr, p, d):
        src = tokq(arr, p * 2 + c, f)
        return rc(src, src, z_ss.at[arr, p, d], tok_rs.at[arr, p, f], plane(1 if d else -1))

    def xy_copy(arr, p, d):
        src = tokq(arr, p * 2 + c, f)
        return rc(src, src, xy_ss.at[arr, p, d], tok_rs.at[arr, p, f], dev_y if d else dev_x)

    def relay_copy(arr, p):
        q = f_y if arr else f_x
        src = tokq(arr, p * 2 + c, q)
        return rc(src, src, dg_ss.at[arr, p], tok_rs.at[arr, p, q], dev_x if arr else dev_y)

    def tok_wait(arr, p, q):
        dst = tokq(arr, p * 2 + c, q)
        rc(dst, dst, z_ss.at[arr, p, 0], tok_rs.at[arr, p, q], dev_x).wait_recv()

    def d2d_copy(arr, p, core):
        src = tok.at[arr, p * 2 + core]
        return rc(src, src, d2d_ss.at[arr, p], d2d_rs.at[arr, p], partner)

    def w_copy(i, to):
        return rc(
            (gate_t, up_t, wd_ref)[i].at[pl.ds(pl.multiple_of(to * hid, hid), hid)],
            wts.at[i, :, own_cols], w_ss.at[i, to], w_rs.at[i, t], {"tp": to},
        )

    def w_send(d):
        @pl.loop(2, 2 * n_z)
        def _(k):
            p = z + k // 2 if d else z - k // 2

            @pl.when((p >= 0) & (p < n_z))
            def _():
                for i in range(3):
                    w_copy(i, p * 2 + k % 2).start()

    for arr in range(2):
        for d, ok in ((1, z < n_z - 1), (0, z > 0)):
            @pl.when(ok)
            def _(arr=arr, d=d):
                z_copy(arr, z, d).start()
        d2d_copy(arr, z, c).start()

    gate_t[...] = wg_ref[...].T
    up_t[...] = wu_ref[...].T
    own_rows = pl.ds(pl.multiple_of(t * hid, hid), hid)
    for i, w in enumerate((gate_t, up_t, wd_ref)):
        wts[i, :, own_cols] = w[own_rows]

    for i in range(3):
        w_copy(i, z * 2 + 1 - c).start()

    for step in range(n_z):
        for d in (1, 0):
            p = z - step if d else z + step

            if step == 0:
                continue

            @pl.when((p >= 0) & (p < n_z))
            def _(p=p, d=d):
                for arr in range(2):
                    tok_wait(arr, p, f)

                    @pl.when(z < n_z - 1 if d else z > 0)
                    def _():
                        z_copy(arr, p, d).start()

                    xy_copy(arr, p, 0).start()
                    xy_copy(arr, p, 1).start()

        for d in (1, 0):
            @pl.when((z if d else n_z - 1 - z) == step)
            def _(d=d):
                w_send(d)

    def order(j):
        return jnp.where(z < n_z // 2, z + j, z - j + n_z) % n_z

    def sweep(j):
        return jnp.where(j % 2 == 0, n_z - 1 - j // 2, j // 2)

    @pl.loop(1, n_z)
    def _(j):
        p = order(j)
        tok_wait(0, p, f_x)
        relay_copy(0, p).start()
        tok_wait(1, p, f_y)
        relay_copy(1, p).start()

    @pl.loop(1, n_z)
    def _(j):
        p = order(j)
        tok_wait(0, p, f_y)
        tok_wait(0, p, f_d)
        d2d_copy(0, p, c).start()
        tok_wait(1, p, f_x)
        tok_wait(1, p, f_d)
        d2d_copy(1, p, c).start()

    for i in range(3):
        for k in range(1, n_tp):
            frm = (t - k + n_tp) % n_tp
            dst = wts.at[i, :, pl.ds(pl.multiple_of(frm * cols, cols), cols)]
            rc(dst, dst, w_ss.at[i, frm], w_rs.at[i, frm], partner).wait_recv()

    acc[...] = jnp.zeros_like(acc)

    def core_copy(p):
        return rc(part.at[p * 2 + 1 - c], core_in.at[p], core_ss.at[p], core_rs.at[p], partner)

    def side(first_x):
        return pl.ds(width // 2 if first_x else 0, width // 2)

    def half_copy(p, first_x, i):
        q = i * 2 + (1 - fx) if first_x else (1 - fy) * 2 + i
        return rc(
            part.at[p * 2 + c, qs(q), side(first_x)], half_in.at[p, i, :, side(first_x)],
            half_ss.at[p, i, int(first_x)], half_rs.at[p, i, int(first_x)],
            dev_x if first_x else dev_y,
        )

    @pl.loop(0, n_z)
    def _(j):
        p = sweep(j)
        for arr in range(2):
            dst = tok.at[arr, p * 2 + 1 - c]
            rc(dst, dst, d2d_ss.at[arr, p], d2d_rs.at[arr, p], partner).wait_recv()

        @pl.loop(0, 2)
        def _(u):
            s = p * 2 + jnp.where(u == 0, 1 - c, c)
            rows, ct = tok[0, s], tok[1, s]
            gate_pre = contract_hidden(rows, wts[0])
            up_pre = contract_hidden(rows, wts[1])
            hidden_grad = contract_hidden(ct, wts[2])
            sig = jax.nn.sigmoid(gate_pre)
            silu = gate_pre * sig
            hidden = (silu * up_pre).astype(BF16)
            gate_grad = (hidden_grad * up_pre * sig * (1.0 + gate_pre * (1.0 - sig))).astype(BF16)
            up_grad = (hidden_grad * silu).astype(BF16)
            acc[...] += contract_tokens(hidden, ct)
            part[s] = (
                jnp.dot(gate_grad, wts[0], preferred_element_type=F32)
                + jnp.dot(up_grad, wts[1], preferred_element_type=F32)
            ).astype(BF16)

            @pl.when(u == 0)
            def _():
                core_copy(p).start()

        core_copy(p).wait_recv()
        s = p * 2 + c
        part[s] = (part[s].astype(F32) + core_in[p].astype(F32)).astype(BF16)
        for i in range(2):
            half_copy(p, True, i).start()
            half_copy(p, False, i).start()

    down_out[...] = acc[...].astype(BF16)

    def dn_copy(k):
        to = (t + k) % n_tp
        return rc(
            down_out.at[:, pl.ds(pl.multiple_of(to * cols, cols), cols)],
            down_in.at[pl.ds(pl.multiple_of(t * hid, hid), hid)],
            dn_ss.at[k], dn_rs.at[k], {"tp": to},
        )

    for k in range(1, n_tp):
        dn_copy(k).start()

    def quarter_copy(p, first_x):
        return rc(
            part.at[p * 2 + c, qs(f_y if first_x else f_x), side(first_x)],
            quarter_in.at[p, :, side(first_x)],
            q_ss.at[p, int(first_x)], q_rs.at[p, int(first_x)], dev_y if first_x else dev_x,
        )

    def half_add(p):
        s = p * 2 + c
        for first_x in (True, False):
            mine = fy if first_x else fx
            half = side(first_x)
            for i in range(2):
                half_copy(p, first_x, i).wait_recv()
            q_other = f_y if first_x else f_x
            part[s, qs(q_other), half] = (
                part[s, qs(q_other), half].astype(F32) + half_in[p, 1 - mine, :, half].astype(F32)
            ).astype(BF16)
            quarter_copy(p, first_x).start()
            part[s, qs(f), half] = (
                part[s, qs(f), half].astype(F32) + half_in[p, mine, :, half].astype(F32)
            ).astype(BF16)

    def chain_copy(p):
        return rc(
            part.at[p * 2 + c, qs(f)], chain_in.at[z], ch_ss.at[p], ch_rs.at[z], {"tp": p * 2 + c}
        )

    @pl.loop(0, n_z + 1)
    def _(j):
        @pl.when(j < n_z)
        def _():
            half_add(sweep(j))

        @pl.when(j > 0)
        def _():
            p = sweep(j - 1)
            quarter_copy(p, True).wait_recv()
            quarter_copy(p, False).wait_recv()
            s = p * 2 + c
            part[s, qs(f)] = (part[s, qs(f)].astype(F32) + quarter_in[p].astype(F32)).astype(BF16)

            @pl.when(p != z)
            def _():
                chain_copy(p).start()

    @pl.loop(0, n_z)
    def _(j):
        frm = sweep(j)

        @pl.when(frm != z)
        def _():
            dst = chain_in.at[frm]
            rc(dst, dst, ch_ss.at[frm], ch_rs.at[frm], partner).wait_recv()
            part[t, qs(f)] = (part[t, qs(f)].astype(F32) + dst[...].astype(F32)).astype(BF16)

    grad_ref[0, qs(f)] = part[t, qs(f)]

    def ag_copy(i, q):
        return rc(
            part.at[t, qs(f)], grad_ref.at[0, qs(q)], ag_ss.at[i], ag_rs.at[i], (dev_x, dev_y, dev_d)[i]
        )

    for i in (2, 0, 1):
        ag_copy(i, f).start()

    down_ref[pl.ds(pl.multiple_of(t * hid, hid), hid)] = acc[:, own_cols]
    for k in range(1, n_tp):
        frm = (t - k + n_tp) % n_tp
        rows = pl.ds(pl.multiple_of(frm * hid, hid), hid)
        rc(down_in.at[rows], down_in.at[rows], dn_ss.at[k], dn_rs.at[k], partner).wait_recv()
        down_ref[rows] = down_in[rows].astype(F32)

    for i, q in enumerate((f_x, f_y, f_d)):
        ag_copy(i, q).wait_recv()

    for arr in range(2):
        for p in range(n_z):
            @pl.when((z < n_z - 1) & (p <= z))
            def _(arr=arr, p=p):
                z_copy(arr, p, 1).wait_send()

            @pl.when((z > 0) & (p >= z))
            def _(arr=arr, p=p):
                z_copy(arr, p, 0).wait_send()

            d2d_copy(arr, p, c).wait_send()

            @pl.when(p != z)
            def _(arr=arr, p=p):
                xy_copy(arr, p, 0).wait_send()
                xy_copy(arr, p, 1).wait_send()
                relay_copy(arr, p).wait_send()

    for k in range(1, n_tp):
        for i in range(3):
            w_copy(i, (t + k) % n_tp).wait_send()
        dn_copy(k).wait_send()
    for p in range(n_z):
        core_copy(p).wait_send()
        for first_x in (True, False):
            half_copy(p, first_x, 0).wait_send()
            half_copy(p, first_x, 1).wait_send()
            quarter_copy(p, first_x).wait_send()

        @pl.when(p != z)
        def _(p=p):
            chain_copy(p).wait_send()

    for i in range(3):
        ag_copy(i, f).wait_send()


def spread(n_tp, inputs, cotangent, gate_weight, up_weight, down_weight):
    _, n_tok, width = inputs.shape
    hid_all = gate_weight.shape[1]
    hid, cols, n_z, qr = hid_all // n_tp, width // n_tp, n_tp // 2, n_tok // 4
    dma = pltpu.SemaphoreType.DMA
    vmem = pl.BlockSpec(memory_space=pltpu.VMEM)
    anyspace = pl.BlockSpec(memory_space=pl.ANY)
    return pl.pallas_call(
        functools.partial(kernel, n_tp),
        name="spread_hidden",
        out_shape=(
            jax.ShapeDtypeStruct((1, n_tok, width), BF16),
            jax.ShapeDtypeStruct((hid_all, cols), F32),
        ),
        in_specs=[anyspace, anyspace, vmem, vmem, vmem],
        out_specs=(vmem, vmem),
        scratch_shapes=[
            pltpu.VMEM((2, n_tp, n_tok, width), BF16),
            pltpu.VMEM((n_tp, n_tok, width), BF16),
            pltpu.VMEM((n_z, n_tok, width), BF16),
            pltpu.VMEM((n_z, 2, qr, width), BF16),
            pltpu.VMEM((n_z, qr, width), BF16),
            pltpu.VMEM((n_z, qr, width), BF16),
            pltpu.VMEM((3, hid, width), BF16),
            pltpu.VMEM((hid, width), F32),
            pltpu.VMEM((hid, width), BF16),
            pltpu.VMEM((hid_all, cols), BF16),
            pltpu.VMEM((hid_all, cols), BF16),
            pltpu.VMEM((hid_all, cols), BF16),
            dma((2,)), dma((2, n_z, 4)), dma((2, n_z, 2)), dma((2, n_z, 2)), dma((2, n_z)),
            dma((2, n_z)), dma((2, n_z)), dma((3, n_tp)), dma((3, n_tp)), dma((n_z,)), dma((n_z,)),
            dma((n_z, 2, 2)), dma((n_z, 2, 2)), dma((n_z, 2)), dma((n_z, 2)), dma((n_z,)), dma((n_z,)),
            dma((3,)), dma((3,)), dma((n_tp,)), dma((n_tp,)),
        ],
        compiler_params=pltpu.CompilerParams(
            collective_id=0, has_side_effects=True, vmem_limit_bytes=66_000_000
        ),
    )(inputs, cotangent, gate_weight, up_weight, down_weight)


def solution(mesh):
    n_fs, n_tp = mesh.shape["fs"], mesh.shape["tp"]

    def per_device(inputs, cotangent, gate_weight, up_weight, down_weight):
        _, n_tok, width = inputs.shape
        hid_all = gate_weight.shape[1]
        n_z = n_tp // 2
        fits = (
            n_fs == 4
            and n_tp % 2 == 0
            and hid_all % (n_tp * 16) == 0
            and width % (n_tp * 128) == 0
            and n_tok % 64 == 0
            and 2 * n_tok * width * (3 * n_tp + 3 * n_z + 4) + 16 * hid_all * width < 62_000_000 * 2
        )
        if not fits:
            return gathered(inputs, cotangent, gate_weight, up_weight, down_weight)
        return spread(n_tp, inputs, cotangent, gate_weight, up_weight, down_weight)

    return jax.shard_map(
        per_device,
        mesh=mesh,
        in_specs=(
            P("tp", None, None),
            P("tp", None, None),
            P("tp", "fs"),
            P("tp", "fs"),
            P("fs", "tp"),
        ),
        out_specs=(P("tp", None, None), P("fs", "tp")),
        check_vma=False,
    )
```

profile of v0, /device:TPU:16, one launch (start us, length us, event | category | flops | bytes accessed | tf_op | source)
XLA Modules:
  0.0 186.6 jit_solution(9930806432001983336)
XLA Ops:
  0.6 182.2 %spread_hidden.1 = (bf16[1,320,2048]{2,1,0:T(8,128)(2,1)}, f32[1408,256]{1,0:T(8,128)}) custom-call(bf16[1,320,2048]{2,1,0:T(8,128)(2,1)} %x_ref.1, bf16[1,320,2048]{2,1,0:T(8,128)(2,1)} %ct_ref.1, bf16[256,1408]{1,0:T(8,128)(2,1)} %wg_ref.1, bf16[256,1408]{1,0:T(8,128)(2,1)} %wu_ref.1, bf16[1408,256]{1,0:T(8,128)(2,1)} %wd_ref.1), custom_call_target="tpu_custom_call" | custom-call | tf_op jit(solution)/shard_map/spread_hidden/pallas_call | solution.py:394
  182.8 0.0 copy-start
  182.8 2.6 %copy.9 = bf16[1,320,2048]{2,1,0:T(8,128)(2,1)} copy(bf16[1,320,2048]{2,1,0:T(8,128)(2,1)} %get-tuple-element.4) | data formatting | bytes 2621440
  185.5 0.0 copy-done
  185.5 1.1 copy.10
Async XLA Ops:
  182.8 2.6 %copy-start = (f32[1408,256]{1,0:T(8,128)S(1)}, f32[1408,256]{1,0:T(8,128)}, u32[]{:S(2)}) copy-start(f32[1408,256]{1,0:T(8,128)} %get-tuple-element.5) | copy-start | bytes 4325380
where the time goes:
time: 187 us
  Pallas kernels  182 us (97%)
  local copies, waits for them, and re-layouts  3.73 us (2%)
    pallas_call x1, Pallas kernels, spread(): pl.pallas_call(functools.partial(kernel, n_tp), name='spread_hidden', out...  182 us

commit v1 on v0

v1 whole, which is shorter than its diff:
```python
import functools

import jax
import jax.numpy as jnp
from jax import lax
from jax.experimental import pallas as pl
from jax.experimental.pallas import tpu as pltpu
from jax.sharding import PartitionSpec as P

MESH = pl.DeviceIdType.MESH
BF16 = jnp.bfloat16
F32 = jnp.float32


def contract_hidden(left, right):
    return lax.dot_general(left, right, (((1,), (1,)), ((), ())), preferred_element_type=F32)


def contract_tokens(left, right):
    return lax.dot_general(left, right, (((0,), (0,)), ((), ())), preferred_element_type=F32)


def gathered(inputs, cotangent, gate_weight, up_weight, down_weight):
    rows_in = inputs[0]
    rows_grad = cotangent[0]
    token_count, model_width = rows_in.shape
    gate_full = lax.all_gather(gate_weight, "tp", axis=0, tiled=True)
    up_full = lax.all_gather(up_weight, "tp", axis=0, tiled=True)
    down_tall = lax.all_gather(down_weight.T, "tp", axis=0, tiled=True)
    gate_pre = jnp.dot(rows_in, gate_full, preferred_element_type=F32)
    up_pre = jnp.dot(rows_in, up_full, preferred_element_type=F32)
    sig = jax.nn.sigmoid(gate_pre)
    hidden = (gate_pre * sig * up_pre).astype(BF16)
    hidden_grad = jnp.dot(rows_grad, down_tall, preferred_element_type=F32)
    gate_grad = (hidden_grad * up_pre * sig * (1.0 + gate_pre * (1.0 - sig))).astype(BF16)
    up_grad = (hidden_grad * gate_pre * sig).astype(BF16)
    partial_down = contract_tokens(hidden, rows_grad)
    down_grad = lax.psum_scatter(
        partial_down.astype(BF16), "tp", scatter_dimension=1, tiled=True
    ).astype(F32)
    own_sum = lax.psum_scatter(
        (contract_hidden(gate_grad, gate_full) + contract_hidden(up_grad, up_full)).astype(BF16),
        "fs",
        scatter_dimension=0,
        tiled=True,
    )
    whole_grad = lax.all_gather(own_sum, "fs", axis=0, tiled=True)
    return (whole_grad.reshape(1, token_count, model_width), down_grad)


def kernel(
    n_tp, x_ref, ct_ref, wg_ref, wu_ref, wd_ref, grad_ref, down_ref,
    tok, wts, gate_t, up_t, part, y_in, z_in, acc, gate_g, up_g,
    dn_out, dn_in, dx_out, dx_in, dz_out, dz_in,
    loc_sem, z_ss, y_ss, tok_zs, tok_ys, w_ss, w_rs, x_ss, x_rs, d_ss, d_rs,
    yi_ss, yi_rs, zi_ss, zi_rs, ag_ss, ag_rs, dn_ss, dn_rs, dx_ss, dx_rs, dz_ss, dz_rs,
):
    f, t = lax.axis_index("fs"), lax.axis_index("tp")
    n_z = n_tp // 2
    z, c = t // 2, t % 2
    fy, fx = f // 2, f % 2
    dev_x, dev_y = {"fs": fy * 2 + 1 - fx}, {"fs": (1 - fy) * 2 + fx}
    partner = {"tp": z * 2 + 1 - c}
    half, width = tok.shape[2], tok.shape[3]
    quarter = half // 2
    hid = wts.shape[1] // 2
    cols = width // n_tp
    weights = (gate_t, up_t, wd_ref)

    def plane(p):
        return {"tp": p * 2 + c}

    def rc(src, dst, ss, rs, dev):
        return pltpu.make_async_remote_copy(
            src_ref=src, dst_ref=dst, send_sem=ss, recv_sem=rs, device_id=dev, device_id_type=MESH
        )

    def ds(index, size):
        return pl.ds(pl.multiple_of(index * size, size), size)

    def near(j):
        low = jnp.where(z < n_z // 2, z, n_z - 1 - z)
        step = jnp.where(j % 2 == 1, (j + 1) // 2, -(j // 2))
        p = jnp.where(j <= 2 * low, low + step, j)
        return jnp.where(z < n_z // 2, p, n_z - 1 - p)

    def z_copy(arr, p, d):
        src = tok.at[arr, p, ds(fy, quarter)]
        to = z + 1 if d else z - 1
        return rc(src, src, z_ss.at[arr, p, d], tok_zs.at[arr, p], plane(to))

    def y_copy(arr, p):
        src = tok.at[arr, p, ds(fy, quarter)]
        return rc(src, src, y_ss.at[arr, p], tok_ys.at[arr, p], dev_y)

    def z_tok_wait(arr, p):
        dst = tok.at[arr, p, ds(fy, quarter)]
        rc(dst, dst, y_ss.at[arr, p], tok_zs.at[arr, p], dev_y).wait_recv()

    def y_tok_wait(arr, p):
        dst = tok.at[arr, p, ds(1 - fy, quarter)]
        rc(dst, dst, y_ss.at[arr, p], tok_ys.at[arr, p], dev_y).wait_recv()

    def tok_in(arr, p):
        z_tok_wait(arr, p)

        @pl.when((p < z) & (z < n_z - 1))
        def _():
            z_copy(arr, p, 1).start()

        @pl.when((p > z) & (z > 0))
        def _():
            z_copy(arr, p, 0).start()

        y_copy(arr, p).start()

    def block(i, side, s, core):
        return wts.at[i, ds(side, hid), ds(s * 2 + core, cols)]

    def own_block(i, p):
        return weights[i].at[ds(p, hid)]

    def w_copy(i, to):
        return rc(own_block(i, to), block(i, fx, z, c), w_ss.at[i, to], w_rs.at[i, z], plane(to))

    def x_copy(i, s, src=None):
        dst = block(i, fx, s, c)
        return rc(dst if src is None else src, dst, x_ss.at[i, s], x_rs.at[i, s], dev_x)

    def d_copy(i, other, s, src=None):
        side = 1 - fx if other else fx
        dst = block(i, side, s, c)
        return rc(
            dst if src is None else src, dst, d_ss.at[i, other, s], d_rs.at[i, other, s], partner
        )

    own = [
        pltpu.make_async_copy(x_ref.at[0, ds(fx, half)], tok.at[0, z], loc_sem.at[0]),
        pltpu.make_async_copy(ct_ref.at[0, ds(fx, half)], tok.at[1, z], loc_sem.at[1]),
    ]
    for copy in own:
        copy.start()

    barrier = pltpu.get_barrier_semaphore()
    for dev in (dev_x, dev_y):
        pl.semaphore_signal(barrier, inc=1, device_id=dev, device_id_type=MESH)
    for k in range(1, n_tp):
        pl.semaphore_signal(barrier, inc=1, device_id={"tp": (t + k) % n_tp}, device_id_type=MESH)
    pl.semaphore_wait(barrier, 2 + n_tp - 1)

    for arr in range(2):
        own[arr].wait()
        for d, ok in ((1, z < n_z - 1), (0, z > 0)):
            @pl.when(ok)
            def _(arr=arr, d=d):
                z_copy(arr, z, d).start()

    def w_send(i):
        x_copy(i, z, own_block(i, z)).start()
        d_copy(i, 0, z, own_block(i, z)).start()
        for j in range(1, n_z):
            w_copy(i, near(j)).start()

    w_send(2)
    gate_t[...] = wg_ref[...].T
    w_send(0)
    up_t[...] = wu_ref[...].T
    w_send(1)
    for i in range(3):
        wts[i, ds(fx, hid), ds(t, cols)] = weights[i][ds(z, hid)]
    acc[...] = jnp.zeros_like(acc)

    for arr in range(2):
        for p, ok in ((z + 1, z < n_z - 1), (z - 1, z > 0)):
            @pl.when(ok)
            def _(arr=arr, p=p):
                tok_in(arr, p)

    def w_in(i):
        @pl.loop(1, n_z)
        def _(j):
            s = near(j)
            dst = block(i, fx, s, c)
            rc(dst, dst, w_ss.at[i, s], w_rs.at[i, s], partner).wait_recv()
            x_copy(i, s).start()
            d_copy(i, 0, s).start()

    def x_in(i):
        @pl.loop(0, n_z)
        def _(j):
            s = jnp.where(j == 0, z, near(j))
            dst = block(i, 1 - fx, s, c)
            rc(dst, dst, x_ss.at[i, s], x_rs.at[i, s], partner).wait_recv()
            d_copy(i, 1, s).start()

    w_in(2)
    x_in(2)
    w_in(0)
    x_in(0)
    w_in(1)
    x_in(1)
    for i in range(3):
        for other in range(2):
            side = 1 - fx if other else fx
            for s in range(n_z):
                dst = block(i, side, s, 1 - c)
                rc(dst, dst, d_ss.at[i, other, s], d_rs.at[i, other, s], partner).wait_recv()

    def yi_copy(p):
        return rc(
            part.at[p, ds(1 - fy, quarter)], y_in.at[p], yi_ss.at[p], yi_rs.at[p], dev_y
        )

    def zi_copy(p):
        return rc(part.at[p, ds(fy, quarter)], z_in.at[z], zi_ss.at[p], zi_rs.at[z], plane(p))

    def sweep(p):
        rows, ct = tok[0, p], tok[1, p]

        @pl.loop(0, 2)
        def _(h):
            hs = ds(h, hid)
            gate_pre = contract_hidden(rows, wts[0, hs])
            up_pre = contract_hidden(rows, wts[1, hs])
            hidden_grad = contract_hidden(ct, wts[2, hs])
            sig = jax.nn.sigmoid(gate_pre)
            silu = gate_pre * sig
            hidden = (silu * up_pre).astype(BF16)
            gate_g[h] = (hidden_grad * up_pre * sig * (1.0 + gate_pre * (1.0 - sig))).astype(BF16)
            up_g[h] = (hidden_grad * silu).astype(BF16)
            for n in range(2):
                at = pl.ds(n * (width // 2), width // 2)
                acc[hs, at] += contract_tokens(hidden, ct[:, n * (width // 2) : (n + 1) * (width // 2)])

        @pl.loop(0, 2)
        def _(n):
            at = ds(n, width // 2)
            total = jnp.dot(gate_g[0], wts[0, :hid, at], preferred_element_type=F32)
            total += jnp.dot(up_g[0], wts[1, :hid, at], preferred_element_type=F32)
            total += jnp.dot(gate_g[1], wts[0, hid:, at], preferred_element_type=F32)
            total += jnp.dot(up_g[1], wts[1, hid:, at], preferred_element_type=F32)
            part[p, :, at] = total.astype(BF16)

    def y_add(p):
        dst = y_in.at[p]
        rc(dst, dst, yi_ss.at[p], yi_rs.at[p], dev_y).wait_recv()
        mine = ds(fy, quarter)
        part[p, mine] = (part[p, mine].astype(F32) + y_in[p].astype(F32)).astype(BF16)

        @pl.when(p != z)
        def _():
            zi_copy(p).start()

    def turn(j):
        return jnp.where(j == n_z - 1, z, near(j + 1))

    @pl.loop(0, n_z)
    def _(j):
        p = turn(j)

        @pl.when((p > z + 1) | (p < z - 1))
        def _():
            for arr in range(2):
                tok_in(arr, p)

        @pl.when(p != z)
        def _():
            for arr in range(2):
                y_tok_wait(arr, p)

        sweep(p)
        yi_copy(p).start()

        @pl.when(j > 0)
        def _():
            y_add(turn(j - 1))

    def far(k):
        return jnp.where(k == n_z - 1, z, near(n_z - 1 - k))

    def dn_copy(p):
        return rc(dn_out.at[p], dn_in.at[p], dn_ss.at[p], dn_rs.at[p], partner)

    def dx_copy(p):
        return rc(dx_out.at[p], dx_in.at[p], dx_ss.at[p], dx_rs.at[p], dev_x)

    def dz_copy(p):
        return rc(dz_out.at[p], dz_in.at[z], dz_ss.at[p], dz_rs.at[z], plane(p))

    @pl.loop(0, n_z)
    def _(k):
        p = far(k)
        dn_out[p] = acc[:, ds(p * 2 + 1 - c, cols)].astype(BF16)
        dn_copy(p).start()

    @pl.loop(0, n_z)
    def _(k):
        p = far(k)
        dn_copy(p).wait_recv()
        mine = ds(p * 2 + c, cols)
        other = ds(1 - fx, hid)
        here = ds(fx, hid)
        dx_out[p] = (acc[other, mine] + dn_in[p, other].astype(F32)).astype(BF16)
        dx_copy(p).start()
        acc[here, mine] = acc[here, mine] + dn_in[p, here].astype(F32)

    @pl.loop(0, n_z)
    def _(k):
        p = far(k)
        dx_copy(p).wait_recv()
        total = acc[ds(fx, hid), ds(p * 2 + c, cols)] + dx_in[p].astype(F32)

        @pl.when(p == z)
        def _():
            down_ref[ds(z, hid)] = total

        @pl.when(p != z)
        def _():
            dz_out[p] = total.astype(BF16)
            dz_copy(p).start()

    y_add(z)

    own_rows = ds(fx * 2 + fy, quarter)
    total = part[z, ds(fy, quarter)].astype(F32)
    for j in range(1, n_z):
        s = near(j)
        dst = z_in.at[s]
        rc(dst, dst, zi_ss.at[s], zi_rs.at[s], partner).wait_recv()
        total += z_in[s].astype(F32)
    grad_ref[0, own_rows] = total.astype(BF16)

    def ag_copy(i, rows, dev):
        src = grad_ref.at[0, rows]
        return rc(src, src, ag_ss.at[i], ag_rs.at[i], dev)

    x_rows = ds((1 - fx) * 2 + fy, quarter)
    y_rows = ds(fx * 2 + 1 - fy, quarter)
    d_rows = ds((1 - fx) * 2 + 1 - fy, quarter)
    ag_copy(0, own_rows, dev_x).start()
    ag_copy(1, own_rows, dev_y).start()
    ag_copy(0, x_rows, dev_x).wait_recv()
    ag_copy(2, x_rows, dev_y).start()

    for j in range(1, n_z):
        s = near(j)
        dst = dz_in.at[s]
        rc(dst, dst, dz_ss.at[s], dz_rs.at[s], partner).wait_recv()
        down_ref[ds(s, hid)] = dz_in[s].astype(F32)

    ag_copy(1, y_rows, dev_y).wait_recv()
    ag_copy(2, d_rows, dev_y).wait_recv()

    for arr in range(2):
        for p in range(n_z):
            @pl.when((z < n_z - 1) & (p <= z))
            def _(arr=arr, p=p):
                z_copy(arr, p, 1).wait_send()

            @pl.when((z > 0) & (p >= z))
            def _(arr=arr, p=p):
                z_copy(arr, p, 0).wait_send()

            @pl.when(p != z)
            def _(arr=arr, p=p):
                y_copy(arr, p).wait_send()

    for p in range(n_z):
        for i in range(3):
            x_copy(i, p).wait_send()
            d_copy(i, 0, p).wait_send()
            d_copy(i, 1, p).wait_send()
        yi_copy(p).wait_send()
        dn_copy(p).wait_send()
        dx_copy(p).wait_send()

        @pl.when(p != z)
        def _(p=p):
            for i in range(3):
                w_copy(i, p).wait_send()
            zi_copy(p).wait_send()
            dz_copy(p).wait_send()

    ag_copy(0, own_rows, dev_x).wait_send()
    ag_copy(1, own_rows, dev_y).wait_send()
    ag_copy(2, x_rows, dev_y).wait_send()


def spread(n_tp, inputs, cotangent, gate_weight, up_weight, down_weight):
    _, n_tok, width = inputs.shape
    hid_all = gate_weight.shape[1]
    n_z = n_tp // 2
    hid, cols, half, quarter = hid_all // n_z, width // n_tp, n_tok // 2, n_tok // 4
    dma = pltpu.SemaphoreType.DMA
    vmem = pl.BlockSpec(memory_space=pltpu.VMEM)
    anyspace = pl.BlockSpec(memory_space=pl.ANY)
    return pl.pallas_call(
        functools.partial(kernel, n_tp),
        name="spread_hidden",
        out_shape=(
            jax.ShapeDtypeStruct((1, n_tok, width), BF16),
            jax.ShapeDtypeStruct((hid_all, cols), F32),
        ),
        in_specs=[anyspace, anyspace, vmem, vmem, vmem],
        out_specs=(vmem, vmem),
        scratch_shapes=[
            pltpu.VMEM((2, n_z, half, width), BF16),
            pltpu.VMEM((3, 2 * hid, width), BF16),
            pltpu.VMEM((hid_all, cols), BF16),
            pltpu.VMEM((hid_all, cols), BF16),
            pltpu.VMEM((n_z, half, width), BF16),
            pltpu.VMEM((n_z, quarter, width), BF16),
            pltpu.VMEM((n_z, quarter, width), BF16),
            pltpu.VMEM((2 * hid, width), F32),
            pltpu.VMEM((2, half, hid), BF16),
            pltpu.VMEM((2, half, hid), BF16),
            pltpu.VMEM((n_z, 2 * hid, cols), BF16),
            pltpu.VMEM((n_z, 2 * hid, cols), BF16),
            pltpu.VMEM((n_z, hid, cols), BF16),
            pltpu.VMEM((n_z, hid, cols), BF16),
            pltpu.VMEM((n_z, hid, cols), BF16),
            pltpu.VMEM((n_z, hid, cols), BF16),
            dma((2,)), dma((2, n_z, 2)), dma((2, n_z)), dma((2, n_z)), dma((2, n_z)),
            dma((3, n_z)), dma((3, n_z)), dma((3, n_z)), dma((3, n_z)),
            dma((3, 2, n_z)), dma((3, 2, n_z)),
            dma((n_z,)), dma((n_z,)), dma((n_z,)), dma((n_z,)), dma((3,)), dma((3,)),
            dma((n_z,)), dma((n_z,)), dma((n_z,)), dma((n_z,)), dma((n_z,)), dma((n_z,)),
        ],
        compiler_params=pltpu.CompilerParams(
            collective_id=0, has_side_effects=True, vmem_limit_bytes=66_000_000
        ),
    )(inputs, cotangent, gate_weight, up_weight, down_weight)


def solution(mesh):
    n_fs, n_tp = mesh.shape["fs"], mesh.shape["tp"]

    def per_device(inputs, cotangent, gate_weight, up_weight, down_weight):
        _, n_tok, width = inputs.shape
        hid_all = gate_weight.shape[1]
        n_z = n_tp // 2
        fits = (
            n_fs == 4
            and n_tp % 2 == 0
            and hid_all % (n_z * 16) == 0
            and width % (n_tp * 128) == 0
            and n_tok % 64 == 0
            and (3 * n_tok + 9 * hid_all) * n_z * width + 18 * hid_all * width < 62_000_000 * n_z
        )
        if not fits:
            return gathered(inputs, cotangent, gate_weight, up_weight, down_weight)
        return spread(n_tp, inputs, cotangent, gate_weight, up_weight, down_weight)

    return jax.shard_map(
        per_device,
        mesh=mesh,
        in_specs=(
            P("tp", None, None),
            P("tp", None, None),
            P("tp", "fs"),
            P("tp", "fs"),
            P("fs", "tp"),
        ),
        out_specs=(P("tp", None, None), P("fs", "tp")),
        check_vma=False,
    )
```

time: 187 us -> 199 us (1.064)
  the two profiles are of different devices: /device:TPU:16 before, /device:TPU:0 now
where the time goes in v1:
time: 199 us
  Pallas kernels  195 us (98%)
  local copies, waits for them, and re-layouts  3.73 us (2%)
    pallas_call x1, Pallas kernels, spread(): pl.pallas_call(functools.partial(kernel, n_tp), name='spread_hidden', out...  195 us

profile of v1, /device:TPU:0, one launch (start us, length us, event | category | flops | bytes accessed | tf_op | source)
XLA Modules:
  0.0 199.0 jit_solution(10512063718494543375)
XLA Ops:
  0.6 194.7 %spread_hidden.1 = (bf16[1,320,2048]{2,1,0:T(8,128)(2,1)}, f32[1408,256]{1,0:T(8,128)}) custom-call(bf16[1,320,2048]{2,1,0:T(8,128)(2,1)} %x_ref.1, bf16[1,320,2048]{2,1,0:T(8,128)(2,1)} %ct_ref.1, bf16[256,1408]{1,0:T(8,128)(2,1)} %wg_ref.1, bf16[256,1408]{1,0:T(8,128)(2,1)} %wu_ref.1, bf16[1408,256]{1,0:T(8,128)(2,1)} %wd_ref.1), custom_call_target="tpu_custom_call" | custom-call | tf_op jit(solution)/shard_map/spread_hidden/pallas_call | solution.py:397
  195.3 0.0 copy-start
  195.3 2.6 %copy.9 = bf16[1,320,2048]{2,1,0:T(8,128)(2,1)} copy(bf16[1,320,2048]{2,1,0:T(8,128)(2,1)} %get-tuple-element.4) | data formatting | bytes 2621440
  197.9 0.0 copy-done
  197.9 1.1 copy.10
Async XLA Ops:
  195.3 2.6 %copy-start = (f32[1408,256]{1,0:T(8,128)S(1)}, f32[1408,256]{1,0:T(8,128)}, u32[]{:S(2)}) copy-start(f32[1408,256]{1,0:T(8,128)} %get-tuple-element.5) | copy-start | bytes 4325380

commit v2 on v1

--- a/solution.py
+++ b/solution.py
@@ -50,8 +50,8 @@
 
 def kernel(
     n_tp, x_ref, ct_ref, wg_ref, wu_ref, wd_ref, grad_ref, down_ref,
-    tok, wts, gate_t, up_t, part, y_in, z_in, acc, gate_g, up_g,
-    dn_out, dn_in, dx_out, dx_in, dz_out, dz_in,
+    tok, wts, gate_t, up_t, part, y_in, z_in, acc, pre, gate_g, up_g, hidden_b,
+    dn_out, dn_in, dx_out, dx_in, dz_out, dz_in, fwd,
     loc_sem, z_ss, y_ss, tok_zs, tok_ys, w_ss, w_rs, x_ss, x_rs, d_ss, d_rs,
     yi_ss, yi_rs, zi_ss, zi_rs, ag_ss, ag_rs, dn_ss, dn_rs, dx_ss, dx_rs, dz_ss, dz_rs,
 ):
@@ -61,9 +61,9 @@
     fy, fx = f // 2, f % 2
     dev_x, dev_y = {"fs": fy * 2 + 1 - fx}, {"fs": (1 - fy) * 2 + fx}
     partner = {"tp": z * 2 + 1 - c}
-    half, width = tok.shape[2], tok.shape[3]
+    half, width = tok.shape[1] // n_z, tok.shape[2]
     quarter = half // 2
-    hid = wts.shape[1] // 2
+    hid = wts.shape[2] // 2
     cols = width // n_tp
     weights = (gate_t, up_t, wd_ref)
 
@@ -84,21 +84,25 @@
         p = jnp.where(j <= 2 * low, low + step, j)
         return jnp.where(z < n_z // 2, p, n_z - 1 - p)
 
+    def tok_rows(arr, p, side):
+        start = pl.multiple_of(p * half + side * quarter, quarter)
+        return tok.at[arr, pl.ds(start, quarter)]
+
     def z_copy(arr, p, d):
-        src = tok.at[arr, p, ds(fy, quarter)]
+        src = tok_rows(arr, p, fy)
         to = z + 1 if d else z - 1
         return rc(src, src, z_ss.at[arr, p, d], tok_zs.at[arr, p], plane(to))
 
     def y_copy(arr, p):
-        src = tok.at[arr, p, ds(fy, quarter)]
+        src = tok_rows(arr, p, fy)
         return rc(src, src, y_ss.at[arr, p], tok_ys.at[arr, p], dev_y)
 
     def z_tok_wait(arr, p):
-        dst = tok.at[arr, p, ds(fy, quarter)]
+        dst = tok_rows(arr, p, fy)
         rc(dst, dst, y_ss.at[arr, p], tok_zs.at[arr, p], dev_y).wait_recv()
 
     def y_tok_wait(arr, p):
-        dst = tok.at[arr, p, ds(1 - fy, quarter)]
+        dst = tok_rows(arr, p, 1 - fy)
         rc(dst, dst, y_ss.at[arr, p], tok_ys.at[arr, p], dev_y).wait_recv()
 
     def tok_in(arr, p):
@@ -115,13 +119,26 @@
         y_copy(arr, p).start()
 
     def block(i, side, s, core):
-        return wts.at[i, ds(side, hid), ds(s * 2 + core, cols)]
+        return wts.at[i, s * 2 + core, ds(side, hid)]
 
     def own_block(i, p):
         return weights[i].at[ds(p, hid)]
 
-    def w_copy(i, to):
-        return rc(own_block(i, to), block(i, fx, z, c), w_ss.at[i, to], w_rs.at[i, z], plane(to))
+    def w_wait(i, s, to):
+        dst = fwd.at[i, s, to]
+        rc(dst, dst, w_ss.at[i, s, to], w_rs.at[i, s, to], partner).wait_recv()
+
+    def w_hop(i, s, to, src):
+        via = jnp.where(to > z, z + 1, z - 1)
+        sems = (w_ss.at[i, s, to], w_rs.at[i, s, to], plane(via))
+
+        @pl.when(via == to)
+        def _():
+            rc(src, block(i, fx, s, c), *sems).start()
+
+        @pl.when(via != to)
+        def _():
+            rc(src, fwd.at[i, s, to], *sems).start()
 
     def x_copy(i, s, src=None):
         dst = block(i, fx, s, c)
@@ -135,8 +152,8 @@
         )
 
     own = [
-        pltpu.make_async_copy(x_ref.at[0, ds(fx, half)], tok.at[0, z], loc_sem.at[0]),
-        pltpu.make_async_copy(ct_ref.at[0, ds(fx, half)], tok.at[1, z], loc_sem.at[1]),
+        pltpu.make_async_copy(x_ref.at[0, ds(fx, half)], tok.at[0, ds(z, half)], loc_sem.at[0]),
+        pltpu.make_async_copy(ct_ref.at[0, ds(fx, half)], tok.at[1, ds(z, half)], loc_sem.at[1]),
     ]
     for copy in own:
         copy.start()
@@ -155,128 +172,215 @@
             def _(arr=arr, d=d):
                 z_copy(arr, z, d).start()
 
-    def w_send(i):
+    order_i = (2, 0, 1)
+
+    def w_own(i):
         x_copy(i, z, own_block(i, z)).start()
         d_copy(i, 0, z, own_block(i, z)).start()
-        for j in range(1, n_z):
-            w_copy(i, near(j)).start()
-
-    w_send(2)
+        for e in range(1, n_z):
+            for to, ok in ((z + e, z + e < n_z), (z - e, z >= e)):
+                if e == 1:
+                    @pl.when(ok)
+                    def _(to=to):
+                        w_hop(i, z, to, own_block(i, to))
+
+    w_own(2)
     gate_t[...] = wg_ref[...].T
-    w_send(0)
+    w_own(0)
     up_t[...] = wu_ref[...].T
-    w_send(1)
+    w_own(1)
+    for e in range(2, n_z):
+        for i in order_i:
+            for to, ok in ((z + e, z + e < n_z), (z - e, z >= e)):
+                @pl.when(ok)
+                def _(i=i, to=to):
+                    w_hop(i, z, to, own_block(i, to))
     for i in range(3):
-        wts[i, ds(fx, hid), ds(t, cols)] = weights[i][ds(z, hid)]
+        wts[i, t, ds(fx, hid)] = weights[i][ds(z, hid)]
     acc[...] = jnp.zeros_like(acc)
-
-    for arr in range(2):
-        for p, ok in ((z + 1, z < n_z - 1), (z - 1, z > 0)):
-            @pl.when(ok)
-            def _(arr=arr, p=p):
-                tok_in(arr, p)
-
-    def w_in(i):
-        @pl.loop(1, n_z)
-        def _(j):
-            s = near(j)
-            dst = block(i, fx, s, c)
-            rc(dst, dst, w_ss.at[i, s], w_rs.at[i, s], partner).wait_recv()
-            x_copy(i, s).start()
-            d_copy(i, 0, s).start()
-
-    def x_in(i):
-        @pl.loop(0, n_z)
-        def _(j):
-            s = jnp.where(j == 0, z, near(j))
-            dst = block(i, 1 - fx, s, c)
-            rc(dst, dst, x_ss.at[i, s], x_rs.at[i, s], partner).wait_recv()
-            d_copy(i, 1, s).start()
-
-    w_in(2)
-    x_in(2)
-    w_in(0)
-    x_in(0)
-    w_in(1)
-    x_in(1)
-    for i in range(3):
+    pre[...] = jnp.zeros_like(pre)
+
+    def sides(g):
+        return ((z - g, z >= g, 1), (z + g, z + g < n_z, -1))
+
+    def w_in(i, s):
+        w_wait(i, s, z)
+        x_copy(i, s).start()
+        d_copy(i, 0, s).start()
+
+    last = jnp.where(z < n_z // 2, n_z - 1, 0)
+
+    def x_in(i, s):
+        dst = block(i, 1 - fx, s, c)
+        rc(dst, dst, x_ss.at[i, s], x_rs.at[i, s], partner).wait_recv()
+        d_copy(i, 1, s).start()
+
+    def unit(p, s):
+        rows = ds(p, half)
+        for i in range(3):
+            total = pre[i, rows]
+            for k in range(2):
+                at = ds(s * 2 + k, cols)
+                total += contract_hidden(tok[1 if i == 2 else 0, rows, at], wts[i, s * 2 + k])
+            pre[i, rows] = total
+
+    def arrived(i, s):
         for other in range(2):
             side = 1 - fx if other else fx
-            for s in range(n_z):
-                dst = block(i, side, s, 1 - c)
-                rc(dst, dst, d_ss.at[i, other, s], d_rs.at[i, other, s], partner).wait_recv()
+            dst = block(i, side, s, 1 - c)
+            rc(dst, dst, d_ss.at[i, other, s], d_rs.at[i, other, s], partner).wait_recv()
+
+    def finish(g):
+        for k, (s, ok, _) in enumerate(sides(g)):
+            @pl.when(ok & (s != last))
+            def _(k=k, s=s):
+                for i in order_i:
+                    x_in(i, s)
+                for arr in range(2):
+                    y_tok_wait(arr, s)
+                for i in order_i:
+                    arrived(i, s)
+                unit(s, s)
+
+                @pl.loop(0, n_z)
+                def _(r):
+                    dist = jnp.where(r > z, r - z, z - r)
+                    known = dist < g
+                    if k == 1:
+                        known = known | (r == z - g)
+
+                    @pl.when(known)
+                    def _():
+                        unit(s, r)
+                        unit(r, s)
+
+    for g in range(1, n_z):
+        for arr in range(2):
+            for s, ok, _ in sides(g):
+                @pl.when(ok)
+                def _(arr=arr, s=s):
+                    tok_in(arr, s)
+        if g == 1:
+            for i in order_i:
+                x_in(i, z)
+                arrived(i, z)
+            unit(z, z)
+        else:
+            finish(g - 1)
+        for i in order_i:
+            for s, ok, _ in sides(g):
+                @pl.when(ok)
+                def _(i=i, s=s):
+                    w_in(i, s)
+        for e in range(1, n_z - g):
+            for i in order_i:
+                for s, ok, step in sides(g):
+                    to = z + step * e
+
+                    @pl.when(ok & (to >= 0) & (to < n_z))
+                    def _(i=i, s=s, to=to):
+                        w_wait(i, s, to)
+                        w_hop(i, s, to, fwd.at[i, s, to])
+    for arr in range(2):
+        y_tok_wait(arr, last)
+
+    @pl.loop(0, n_z)
+    def _(r):
+        @pl.when(r != last)
+        def _():
+            unit(last, r)
+
+    def whole(i):
+        arrived(i, last)
+
+        @pl.loop(0, n_z // 2)
+        def _(m):
+            rows = ds(m, 2 * half)
+            total = pre[i, rows]
+            for k in range(2):
+                at = ds(last * 2 + k, cols)
+                total += contract_hidden(tok[1 if i == 2 else 0, rows, at], wts[i, last * 2 + k])
+            pre[i, rows] = total
+
+    x_in(2, last)
+    x_in(0, last)
+    whole(2)
+    x_in(1, last)
+    whole(0)
+    whole(1)
 
     def yi_copy(p):
         return rc(
             part.at[p, ds(1 - fy, quarter)], y_in.at[p], yi_ss.at[p], yi_rs.at[p], dev_y
         )
 
+    top = z // (n_z // 2)
+
     def zi_copy(p):
-        return rc(part.at[p, ds(fy, quarter)], z_in.at[z], zi_ss.at[p], zi_rs.at[z], plane(p))
+        away = p // (n_z // 2) != top
+        step = jnp.where(p > z, z + 1, z - 1)
+        to = jnp.where(away & (step // (n_z // 2) != top), p, step)
+        slot = jnp.where(to != p, p, jnp.where(away, n_z + 1, jnp.where(p < z, n_z, p)))
+        return rc(part.at[p, ds(fy, quarter)], z_in.at[slot], zi_ss.at[p], zi_rs.at[slot], plane(to))
+
+    def zi_wait(slot):
+        dst = z_in.at[slot]
+        rc(dst, dst, zi_ss.at[0], zi_rs.at[slot], partner).wait_recv()
 
     def sweep(p):
-        rows, ct = tok[0, p], tok[1, p]
-
-        @pl.loop(0, 2)
-        def _(h):
-            hs = ds(h, hid)
-            gate_pre = contract_hidden(rows, wts[0, hs])
-            up_pre = contract_hidden(rows, wts[1, hs])
-            hidden_grad = contract_hidden(ct, wts[2, hs])
+        @pl.loop(0, half // 32)
+        def _(r):
+            at = ds(p * (half // 32) + r, 32)
+            to = ds(r, 32)
+            gate_pre, up_pre, hidden_grad = pre[0, at], pre[1, at], pre[2, at]
             sig = jax.nn.sigmoid(gate_pre)
             silu = gate_pre * sig
-            hidden = (silu * up_pre).astype(BF16)
-            gate_g[h] = (hidden_grad * up_pre * sig * (1.0 + gate_pre * (1.0 - sig))).astype(BF16)
-            up_g[h] = (hidden_grad * silu).astype(BF16)
-            for n in range(2):
-                at = pl.ds(n * (width // 2), width // 2)
-                acc[hs, at] += contract_tokens(hidden, ct[:, n * (width // 2) : (n + 1) * (width // 2)])
+            hidden_b[to] = (silu * up_pre).astype(BF16)
+            gate_g[to] = (hidden_grad * up_pre * sig * (1.0 + gate_pre * (1.0 - sig))).astype(BF16)
+            up_g[to] = (hidden_grad * silu).astype(BF16)
+
+        @pl.loop(0, n_tp)
+        def _(n):
+            part[p, :, ds(n, cols)] = (
+                jnp.dot(gate_g[...], wts[0, n], preferred_element_type=F32)
+                + jnp.dot(up_g[...], wts[1, n], preferred_element_type=F32)
+            ).astype(BF16)
+
+        yi_copy(p).start()
 
         @pl.loop(0, 2)
         def _(n):
             at = ds(n, width // 2)
-            total = jnp.dot(gate_g[0], wts[0, :hid, at], preferred_element_type=F32)
-            total += jnp.dot(up_g[0], wts[1, :hid, at], preferred_element_type=F32)
-            total += jnp.dot(gate_g[1], wts[0, hid:, at], preferred_element_type=F32)
-            total += jnp.dot(up_g[1], wts[1, hid:, at], preferred_element_type=F32)
-            part[p, :, at] = total.astype(BF16)
+            acc[:, at] += contract_tokens(hidden_b[...], tok[1, ds(p, half), at])
 
     def y_add(p):
         dst = y_in.at[p]
         rc(dst, dst, yi_ss.at[p], yi_rs.at[p], dev_y).wait_recv()
-        mine = ds(fy, quarter)
-        part[p, mine] = (part[p, mine].astype(F32) + y_in[p].astype(F32)).astype(BF16)
 
         @pl.when(p != z)
         def _():
+            mine = ds(fy, quarter)
+            part[p, mine] = (part[p, mine].astype(F32) + y_in[p].astype(F32)).astype(BF16)
+
+            up = jnp.where(p > z, z - 1, z + 1)
+
+            @pl.when((up >= 0) & (up < n_z) & (up // (n_z // 2) == top))
+            def _():
+                zi_wait(p)
+                part[p, mine] = (part[p, mine].astype(F32) + z_in[p].astype(F32)).astype(BF16)
+
             zi_copy(p).start()
 
-    def turn(j):
-        return jnp.where(j == n_z - 1, z, near(j + 1))
+    def far(k):
+        return jnp.where(k == n_z - 1, z, near(n_z - 1 - k))
 
     @pl.loop(0, n_z)
     def _(j):
-        p = turn(j)
-
-        @pl.when((p > z + 1) | (p < z - 1))
-        def _():
-            for arr in range(2):
-                tok_in(arr, p)
-
-        @pl.when(p != z)
-        def _():
-            for arr in range(2):
-                y_tok_wait(arr, p)
-
-        sweep(p)
-        yi_copy(p).start()
-
-        @pl.when(j > 0)
-        def _():
-            y_add(turn(j - 1))
-
-    def far(k):
-        return jnp.where(k == n_z - 1, z, near(n_z - 1 - k))
+        sweep(far(j))
+
+        @pl.when(j == 2)
+        def _():
+            y_add(far(0))
 
     def dn_copy(p):
         return rc(dn_out.at[p], dn_in.at[p], dn_ss.at[p], dn_rs.at[p], partner)
@@ -304,9 +408,7 @@
         dx_copy(p).start()
         acc[here, mine] = acc[here, mine] + dn_in[p, here].astype(F32)
 
-    @pl.loop(0, n_z)
-    def _(k):
-        p = far(k)
+    def dx_add(p):
         dx_copy(p).wait_recv()
         total = acc[ds(fx, hid), ds(p * 2 + c, cols)] + dx_in[p].astype(F32)
 
@@ -319,28 +421,43 @@
             dz_out[p] = total.astype(BF16)
             dz_copy(p).start()
 
-    y_add(z)
+    @pl.loop(1, n_z)
+    def _(k):
+        dx_add(far(k - 1))
+        y_add(far(k))
 
     own_rows = ds(fx * 2 + fy, quarter)
-    total = part[z, ds(fy, quarter)].astype(F32)
-    for j in range(1, n_z):
-        s = near(j)
-        dst = z_in.at[s]
-        rc(dst, dst, zi_ss.at[s], zi_rs.at[s], partner).wait_recv()
-        total += z_in[s].astype(F32)
+    def gain(slot):
+        zi_wait(slot)
+        y_in[z] = (y_in[z].astype(F32) + z_in[slot].astype(F32)).astype(BF16)
+
+    @pl.when((z > 0) & ((z - 1) // (n_z // 2) == top))
+    def _():
+        gain(z)
+
+    @pl.when((z < n_z - 1) & ((z + 1) // (n_z // 2) == top))
+    def _():
+        gain(n_z)
+
+    gain(n_z + 1)
+    total = part[z, ds(fy, quarter)].astype(F32) + y_in[z].astype(F32)
     grad_ref[0, own_rows] = total.astype(BF16)
-
-    def ag_copy(i, rows, dev):
-        src = grad_ref.at[0, rows]
-        return rc(src, src, ag_ss.at[i], ag_rs.at[i], dev)
+    span = width // 4
+
+    def ag_copy(i, n, rows, dev):
+        src = grad_ref.at[0, rows, pl.ds(n * span, span)]
+        return rc(src, src, ag_ss.at[i, n], ag_rs.at[i, n], dev)
 
     x_rows = ds((1 - fx) * 2 + fy, quarter)
     y_rows = ds(fx * 2 + 1 - fy, quarter)
     d_rows = ds((1 - fx) * 2 + 1 - fy, quarter)
-    ag_copy(0, own_rows, dev_x).start()
-    ag_copy(1, own_rows, dev_y).start()
-    ag_copy(0, x_rows, dev_x).wait_recv()
-    ag_copy(2, x_rows, dev_y).start()
+    for n in range(4):
+        ag_copy(1, n, own_rows, dev_y).start()
+        ag_copy(0, n, own_rows, dev_x).start()
+    dx_add(z)
+    for n in range(4):
+        ag_copy(1, n, y_rows, dev_y).wait_recv()
+        ag_copy(2, n, y_rows, dev_x).start()
 
     for j in range(1, n_z):
         s = near(j)
@@ -348,8 +465,9 @@
         rc(dst, dst, dz_ss.at[s], dz_rs.at[s], partner).wait_recv()
         down_ref[ds(s, hid)] = dz_in[s].astype(F32)
 
-    ag_copy(1, y_rows, dev_y).wait_recv()
-    ag_copy(2, d_rows, dev_y).wait_recv()
+    for n in range(4):
+        ag_copy(0, n, x_rows, dev_x).wait_recv()
+        ag_copy(2, n, d_rows, dev_x).wait_recv()
 
     for arr in range(2):
         for p in range(n_z):
@@ -376,14 +494,24 @@
 
         @pl.when(p != z)
         def _(p=p):
-            for i in range(3):
-                w_copy(i, p).wait_send()
             zi_copy(p).wait_send()
             dz_copy(p).wait_send()
 
-    ag_copy(0, own_rows, dev_x).wait_send()
-    ag_copy(1, own_rows, dev_y).wait_send()
-    ag_copy(2, x_rows, dev_y).wait_send()
+    for s in range(n_z):
+        for to in range(n_z):
+            if s == to:
+                continue
+
+            @pl.when((z >= s) & (z < to) if s < to else (z <= s) & (z > to))
+            def _(s=s, to=to):
+                for i in range(3):
+                    src = fwd.at[i, s, to]
+                    rc(src, src, w_ss.at[i, s, to], w_rs.at[i, s, to], partner).wait_send()
+
+    for n in range(4):
+        ag_copy(0, n, own_rows, dev_x).wait_send()
+        ag_copy(1, n, own_rows, dev_y).wait_send()
+        ag_copy(2, n, y_rows, dev_x).wait_send()
 
 
 def spread(n_tp, inputs, cotangent, gate_weight, up_weight, down_weight):
@@ -404,26 +532,29 @@
         in_specs=[anyspace, anyspace, vmem, vmem, vmem],
         out_specs=(vmem, vmem),
         scratch_shapes=[
-            pltpu.VMEM((2, n_z, half, width), BF16),
-            pltpu.VMEM((3, 2 * hid, width), BF16),
+            pltpu.VMEM((2, n_z * half, width), BF16),
+            pltpu.VMEM((3, n_tp, 2 * hid, cols), BF16),
             pltpu.VMEM((hid_all, cols), BF16),
             pltpu.VMEM((hid_all, cols), BF16),
             pltpu.VMEM((n_z, half, width), BF16),
             pltpu.VMEM((n_z, quarter, width), BF16),
-            pltpu.VMEM((n_z, quarter, width), BF16),
+            pltpu.VMEM((n_z + 2, quarter, width), BF16),
             pltpu.VMEM((2 * hid, width), F32),
-            pltpu.VMEM((2, half, hid), BF16),
-            pltpu.VMEM((2, half, hid), BF16),
+            pltpu.VMEM((3, n_z * half, 2 * hid), F32),
+            pltpu.VMEM((half, 2 * hid), BF16),
+            pltpu.VMEM((half, 2 * hid), BF16),
+            pltpu.VMEM((half, 2 * hid), BF16),
             pltpu.VMEM((n_z, 2 * hid, cols), BF16),
             pltpu.VMEM((n_z, 2 * hid, cols), BF16),
             pltpu.VMEM((n_z, hid, cols), BF16),
             pltpu.VMEM((n_z, hid, cols), BF16),
             pltpu.VMEM((n_z, hid, cols), BF16),
             pltpu.VMEM((n_z, hid, cols), BF16),
+            pltpu.VMEM((3, n_z, n_z, hid, cols), BF16),
             dma((2,)), dma((2, n_z, 2)), dma((2, n_z)), dma((2, n_z)), dma((2, n_z)),
-            dma((3, n_z)), dma((3, n_z)), dma((3, n_z)), dma((3, n_z)),
+            dma((3, n_z, n_z)), dma((3, n_z, n_z)), dma((3, n_z)), dma((3, n_z)),
             dma((3, 2, n_z)), dma((3, 2, n_z)),
-            dma((n_z,)), dma((n_z,)), dma((n_z,)), dma((n_z,)), dma((3,)), dma((3,)),
+            dma((n_z,)), dma((n_z,)), dma((n_z,)), dma((n_z + 2,)), dma((3, 4)), dma((3, 4)),
             dma((n_z,)), dma((n_z,)), dma((n_z,)), dma((n_z,)), dma((n_z,)), dma((n_z,)),
         ],
         compiler_params=pltpu.CompilerParams(

time: 199 us -> 167 us (0.84)
  Pallas kernels: 195 us -> 161 us
    pallas_call x1, Pallas kernels: 195 us -> 161 us  [spread(): pl.pallas_call(functools.partial(kernel, n_tp), name='spread_hidden', out...]
where the time goes in v2:
time: 167 us; the launch traced here: 166 us
  Pallas kernels  161 us (96%)
  local copies, waits for them, and re-layouts  3.73 us (2%)
    pallas_call x1, Pallas kernels, spread(): pl.pallas_call(functools.partial(kernel, n_tp), name='spread_hidden', out...  161 us
    unnamed x4, local copies, waits for them, and re-layouts  3.73 us

profile of v2, /device:TPU:0, one launch (start us, length us, event | category | flops | bytes accessed | tf_op | source)
XLA Modules:
  0.0 165.5 jit_solution(8940293466959112546)
XLA Ops:
  0.6 161.1 %spread_hidden.1 = (bf16[1,320,2048]{2,1,0:T(8,128)(2,1)}, f32[1408,256]{1,0:T(8,128)}) custom-call(bf16[1,320,2048]{2,1,0:T(8,128)(2,1)} %x_ref.1, bf16[1,320,2048]{2,1,0:T(8,128)(2,1)} %ct_ref.1, bf16[256,1408]{1,0:T(8,128)(2,1)} %wg_ref.1, bf16[256,1408]{1,0:T(8,128)(2,1)} %wu_ref.1, bf16[1408,256]{1,0:T(8,128)(2,1)} %wd_ref.1), custom_call_target="tpu_custom_call" | custom-call | tf_op jit(solution)/shard_map/spread_hidden/pallas_call | solution.py:525
  161.8 0.0 copy-start
  161.8 2.6 %copy.9 = bf16[1,320,2048]{2,1,0:T(8,128)(2,1)} copy(bf16[1,320,2048]{2,1,0:T(8,128)(2,1)} %get-tuple-element.4) | data formatting | bytes 2621440
  164.4 0.0 copy-done
  164.4 1.1 copy.10
Async XLA Ops:
  161.8 2.6 %copy-start = (f32[1408,256]{1,0:T(8,128)S(1)}, f32[1408,256]{1,0:T(8,128)}, u32[]{:S(2)}) copy-start(f32[1408,256]{1,0:T(8,128)} %get-tuple-element.5) | copy-start | bytes 4325380

commit v3 on v2

--- a/solution.py
+++ b/solution.py
@@ -50,7 +50,7 @@
 
 def kernel(
     n_tp, x_ref, ct_ref, wg_ref, wu_ref, wd_ref, grad_ref, down_ref,
-    tok, wts, gate_t, up_t, part, y_in, z_in, acc, pre, gate_g, up_g, hidden_b,
+    tok, wts, gate_t, up_t, part, y_in, z_in, acc, pre, gate_g, up_g, hidden_b, total,
     dn_out, dn_in, dx_out, dx_in, dz_out, dz_in, fwd,
     loc_sem, z_ss, y_ss, tok_zs, tok_ys, w_ss, w_rs, x_ss, x_rs, d_ss, d_rs,
     yi_ss, yi_rs, zi_ss, zi_rs, ag_ss, ag_rs, dn_ss, dn_rs, dx_ss, dx_rs, dz_ss, dz_rs,
@@ -309,23 +309,32 @@
     whole(0)
     whole(1)
 
-    def yi_copy(p):
+    n_cut = 4
+    cut = width // n_cut
+
+    def yi_copy(p, n):
+        at = ds(n, cut)
         return rc(
-            part.at[p, ds(1 - fy, quarter)], y_in.at[p], yi_ss.at[p], yi_rs.at[p], dev_y
+            part.at[p, ds(1 - fy, quarter), at], y_in.at[p, :, at],
+            yi_ss.at[p, n], yi_rs.at[p, n], dev_y,
         )
 
     top = z // (n_z // 2)
 
-    def zi_copy(p):
+    def zi_copy(p, n):
         away = p // (n_z // 2) != top
         step = jnp.where(p > z, z + 1, z - 1)
         to = jnp.where(away & (step // (n_z // 2) != top), p, step)
         slot = jnp.where(to != p, p, jnp.where(away, n_z + 1, jnp.where(p < z, n_z, p)))
-        return rc(part.at[p, ds(fy, quarter)], z_in.at[slot], zi_ss.at[p], zi_rs.at[slot], plane(to))
-
-    def zi_wait(slot):
-        dst = z_in.at[slot]
-        rc(dst, dst, zi_ss.at[0], zi_rs.at[slot], partner).wait_recv()
+        at = ds(n, cut)
+        return rc(
+            part.at[p, ds(fy, quarter), at], z_in.at[slot, :, at],
+            zi_ss.at[p, n], zi_rs.at[slot, n], plane(to),
+        )
+
+    def zi_wait(slot, n):
+        dst = z_in.at[slot, :, ds(n, cut)]
+        rc(dst, dst, zi_ss.at[0, n], zi_rs.at[slot, n], partner).wait_recv()
 
     def sweep(p):
         @pl.loop(0, half // 32)
@@ -339,46 +348,55 @@
             gate_g[to] = (hidden_grad * up_pre * sig * (1.0 + gate_pre * (1.0 - sig))).astype(BF16)
             up_g[to] = (hidden_grad * silu).astype(BF16)
 
-        @pl.loop(0, n_tp)
+        @pl.loop(0, n_cut)
         def _(n):
-            part[p, :, ds(n, cols)] = (
-                jnp.dot(gate_g[...], wts[0, n], preferred_element_type=F32)
-                + jnp.dot(up_g[...], wts[1, n], preferred_element_type=F32)
-            ).astype(BF16)
-
-        yi_copy(p).start()
+            for k in range(n_tp // n_cut):
+                m = n * (n_tp // n_cut) + k
+                part[p, :, ds(m, cols)] = (
+                    jnp.dot(gate_g[...], wts[0, m], preferred_element_type=F32)
+                    + jnp.dot(up_g[...], wts[1, m], preferred_element_type=F32)
+                ).astype(BF16)
+            yi_copy(p, n).start()
 
         @pl.loop(0, 2)
         def _(n):
             at = ds(n, width // 2)
             acc[:, at] += contract_tokens(hidden_b[...], tok[1, ds(p, half), at])
 
+    mine = ds(fy, quarter)
+
+    def yi_wait(p, n):
+        dst = y_in.at[p, :, ds(n, cut)]
+        rc(dst, dst, yi_ss.at[p, n], yi_rs.at[p, n], dev_y).wait_recv()
+
     def y_add(p):
-        dst = y_in.at[p]
-        rc(dst, dst, yi_ss.at[p], yi_rs.at[p], dev_y).wait_recv()
-
-        @pl.when(p != z)
-        def _():
-            mine = ds(fy, quarter)
-            part[p, mine] = (part[p, mine].astype(F32) + y_in[p].astype(F32)).astype(BF16)
-
-            up = jnp.where(p > z, z - 1, z + 1)
-
-            @pl.when((up >= 0) & (up < n_z) & (up // (n_z // 2) == top))
+        up = jnp.where(p > z, z - 1, z + 1)
+        more = (up >= 0) & (up < n_z) & (up // (n_z // 2) == top)
+
+        @pl.loop(0, n_cut)
+        def _(n):
+            at = ds(n, cut)
+            yi_wait(p, n)
+            total = part[p, mine, at].astype(F32) + y_in[p, :, at].astype(F32)
+            part[p, mine, at] = total.astype(BF16)
+
+            @pl.when(more)
             def _():
-                zi_wait(p)
-                part[p, mine] = (part[p, mine].astype(F32) + z_in[p].astype(F32)).astype(BF16)
-
-            zi_copy(p).start()
+                zi_wait(p, n)
+                part[p, mine, at] = (total + z_in[p, :, at].astype(F32)).astype(BF16)
+
+            zi_copy(p, n).start()
 
     def far(k):
         return jnp.where(k == n_z - 1, z, near(n_z - 1 - k))
+
+    outer = (z == 0) | (z == n_z - 1)
 
     @pl.loop(0, n_z)
     def _(j):
         sweep(far(j))
 
-        @pl.when(j == 2)
+        @pl.when((j == n_z - 2) & outer)
         def _():
             y_add(far(0))
 
@@ -421,41 +439,50 @@
             dz_out[p] = total.astype(BF16)
             dz_copy(p).start()
 
-    @pl.loop(1, n_z)
-    def _(k):
-        dx_add(far(k - 1))
+    y_add(far(1))
+
+    @pl.when(jnp.logical_not(outer))
+    def _():
+        y_add(far(0))
+
+    for k in range(2, n_z - 1):
         y_add(far(k))
+    for k in range(n_z - 1):
+        dx_add(far(k))
 
     own_rows = ds(fx * 2 + fy, quarter)
-    def gain(slot):
-        zi_wait(slot)
-        y_in[z] = (y_in[z].astype(F32) + z_in[slot].astype(F32)).astype(BF16)
-
-    @pl.when((z > 0) & ((z - 1) // (n_z // 2) == top))
-    def _():
-        gain(z)
-
-    @pl.when((z < n_z - 1) & ((z + 1) // (n_z // 2) == top))
-    def _():
-        gain(n_z)
-
-    gain(n_z + 1)
-    total = part[z, ds(fy, quarter)].astype(F32) + y_in[z].astype(F32)
-    grad_ref[0, own_rows] = total.astype(BF16)
-    span = width // 4
-
-    def ag_copy(i, n, rows, dev):
-        src = grad_ref.at[0, rows, pl.ds(n * span, span)]
-        return rc(src, src, ag_ss.at[i, n], ag_rs.at[i, n], dev)
-
     x_rows = ds((1 - fx) * 2 + fy, quarter)
     y_rows = ds(fx * 2 + 1 - fy, quarter)
     d_rows = ds((1 - fx) * 2 + 1 - fy, quarter)
-    for n in range(4):
+
+    def ag_copy(i, n, rows, dev):
+        src = grad_ref.at[0, rows, ds(n, cut)]
+        return rc(src, src, ag_ss.at[i, n], ag_rs.at[i, n], dev)
+
+    below = (z > 0) & ((z - 1) // (n_z // 2) == top)
+    above = (z < n_z - 1) & ((z + 1) // (n_z // 2) == top)
+
+    @pl.loop(0, n_cut)
+    def _(n):
+        at = ds(n, cut)
+
+        def gain(slot):
+            zi_wait(slot, n)
+            total[...] += z_in[slot, :, at].astype(F32)
+
+        yi_wait(z, n)
+        total[...] = part[z, mine, at].astype(F32) + y_in[z, :, at].astype(F32)
+        gain(n_z + 1)
+        pl.when(below)(lambda: gain(z))
+        pl.when(above)(lambda: gain(n_z))
+        grad_ref[0, own_rows, at] = total[...].astype(BF16)
         ag_copy(1, n, own_rows, dev_y).start()
         ag_copy(0, n, own_rows, dev_x).start()
+
     dx_add(z)
-    for n in range(4):
+
+    @pl.loop(0, n_cut)
+    def _(n):
         ag_copy(1, n, y_rows, dev_y).wait_recv()
         ag_copy(2, n, y_rows, dev_x).start()
 
@@ -465,7 +492,7 @@
         rc(dst, dst, dz_ss.at[s], dz_rs.at[s], partner).wait_recv()
         down_ref[ds(s, hid)] = dz_in[s].astype(F32)
 
-    for n in range(4):
+    for n in range(n_cut):
         ag_copy(0, n, x_rows, dev_x).wait_recv()
         ag_copy(2, n, d_rows, dev_x).wait_recv()
 
@@ -488,13 +515,15 @@
             x_copy(i, p).wait_send()
             d_copy(i, 0, p).wait_send()
             d_copy(i, 1, p).wait_send()
-        yi_copy(p).wait_send()
+        for n in range(n_cut):
+            yi_copy(p, n).wait_send()
         dn_copy(p).wait_send()
         dx_copy(p).wait_send()
 
         @pl.when(p != z)
         def _(p=p):
-            zi_copy(p).wait_send()
+            for n in range(n_cut):
+                zi_copy(p, n).wait_send()
             dz_copy(p).wait_send()
 
     for s in range(n_z):
@@ -508,7 +537,7 @@
                     src = fwd.at[i, s, to]
                     rc(src, src, w_ss.at[i, s, to], w_rs.at[i, s, to], partner).wait_send()
 
-    for n in range(4):
+    for n in range(n_cut):
         ag_copy(0, n, own_rows, dev_x).wait_send()
         ag_copy(1, n, own_rows, dev_y).wait_send()
         ag_copy(2, n, y_rows, dev_x).wait_send()
@@ -544,6 +573,7 @@
             pltpu.VMEM((half, 2 * hid), BF16),
             pltpu.VMEM((half, 2 * hid), BF16),
             pltpu.VMEM((half, 2 * hid), BF16),
+            pltpu.VMEM((quarter, width // 4), F32),
             pltpu.VMEM((n_z, 2 * hid, cols), BF16),
             pltpu.VMEM((n_z, 2 * hid, cols), BF16),
             pltpu.VMEM((n_z, hid, cols), BF16),
@@ -554,7 +584,7 @@
             dma((2,)), dma((2, n_z, 2)), dma((2, n_z)), dma((2, n_z)), dma((2, n_z)),
             dma((3, n_z, n_z)), dma((3, n_z, n_z)), dma((3, n_z)), dma((3, n_z)),
             dma((3, 2, n_z)), dma((3, 2, n_z)),
-            dma((n_z,)), dma((n_z,)), dma((n_z,)), dma((n_z + 2,)), dma((3, 4)), dma((3, 4)),
+            dma((n_z, 4)), dma((n_z, 4)), dma((n_z, 4)), dma((n_z + 2, 4)), dma((3, 4)), dma((3, 4)),
             dma((n_z,)), dma((n_z,)), dma((n_z,)), dma((n_z,)), dma((n_z,)), dma((n_z,)),
         ],
         compiler_params=pltpu.CompilerParams(

time: 167 us -> 151 us (0.904)
  Pallas kernels: 161 us -> 146 us
    pallas_call x1, Pallas kernels: 161 us -> 146 us  [spread(): pl.pallas_call(functools.partial(kernel, n_tp), name='spread_hidden', out...]
where the time goes in v3:
time: 151 us
  Pallas kernels  146 us (97%)
  local copies, waits for them, and re-layouts  3.73 us (2%)
    pallas_call x1, Pallas kernels, spread(): pl.pallas_call(functools.partial(kernel, n_tp), name='spread_hidden', out...  146 us
    unnamed x4, local copies, waits for them, and re-layouts  3.73 us

profile of v3, /device:TPU:0, one launch (start us, length us, event | category | flops | bytes accessed | tf_op | source)
XLA Modules:
  0.0 150.8 jit_solution(3409189010155315430)
XLA Ops:
  0.6 146.4 %spread_hidden.1 = (bf16[1,320,2048]{2,1,0:T(8,128)(2,1)}, f32[1408,256]{1,0:T(8,128)}) custom-call(bf16[1,320,2048]{2,1,0:T(8,128)(2,1)} %x_ref.1, bf16[1,320,2048]{2,1,0:T(8,128)(2,1)} %ct_ref.1, bf16[256,1408]{1,0:T(8,128)(2,1)} %wg_ref.1, bf16[256,1408]{1,0:T(8,128)(2,1)} %wu_ref.1, bf16[1408,256]{1,0:T(8,128)(2,1)} %wd_ref.1), custom_call_target="tpu_custom_call" | custom-call | tf_op jit(solution)/shard_map/spread_hidden/pallas_call | solution.py:554
  147.1 0.0 copy-start
  147.1 2.6 %copy.9 = bf16[1,320,2048]{2,1,0:T(8,128)(2,1)} copy(bf16[1,320,2048]{2,1,0:T(8,128)(2,1)} %get-tuple-element.4) | data formatting | bytes 2621440
  149.7 0.0 copy-done
  149.7 1.1 copy.10
Async XLA Ops:
  147.1 2.6 %copy-start = (f32[1408,256]{1,0:T(8,128)S(1)}, f32[1408,256]{1,0:T(8,128)}, u32[]{:S(2)}) copy-start(f32[1408,256]{1,0:T(8,128)} %get-tuple-element.5) | copy-start | bytes 4325380

commit v4 on v3

--- a/solution.py
+++ b/solution.py
@@ -49,10 +49,11 @@
 
 
 def kernel(
-    n_tp, x_ref, ct_ref, wg_ref, wu_ref, wd_ref, grad_ref, down_ref,
+    n_tp, x_ref, ct_ref, wg_hbm, wu_hbm, wd_hbm, grad_hbm, down_hbm,
+    wg_ref, wu_ref, wd_ref, grad_ref, down_ref,
     tok, wts, gate_t, up_t, part, y_in, z_in, acc, pre, gate_g, up_g, hidden_b, total,
     dn_out, dn_in, dx_out, dx_in, dz_out, dz_in, fwd,
-    loc_sem, z_ss, y_ss, tok_zs, tok_ys, w_ss, w_rs, x_ss, x_rs, d_ss, d_rs,
+    loc_sem, out_sem, z_ss, y_ss, tok_zs, tok_ys, w_ss, w_rs, x_ss, x_rs, d_ss, d_rs,
     yi_ss, yi_rs, zi_ss, zi_rs, ag_ss, ag_rs, dn_ss, dn_rs, dx_ss, dx_rs, dz_ss, dz_rs,
 ):
     f, t = lax.axis_index("fs"), lax.axis_index("tp")
@@ -155,7 +156,12 @@
         pltpu.make_async_copy(x_ref.at[0, ds(fx, half)], tok.at[0, ds(z, half)], loc_sem.at[0]),
         pltpu.make_async_copy(ct_ref.at[0, ds(fx, half)], tok.at[1, ds(z, half)], loc_sem.at[1]),
     ]
-    for copy in own:
+    load = [
+        pltpu.make_async_copy(wd_hbm, wd_ref, loc_sem.at[2]),
+        pltpu.make_async_copy(wg_hbm, wg_ref, loc_sem.at[3]),
+        pltpu.make_async_copy(wu_hbm, wu_ref, loc_sem.at[4]),
+    ]
+    for copy in own + load:
         copy.start()
 
     barrier = pltpu.get_barrier_semaphore()
@@ -184,12 +190,15 @@
                     def _(to=to):
                         w_hop(i, z, to, own_block(i, to))
 
+    load[0].wait()
     w_own(2)
+    load[1].wait()
     gate_t[...] = wg_ref[...].T
     w_own(0)
+    load[2].wait()
     up_t[...] = wu_ref[...].T
     w_own(1)
-    for e in range(2, n_z):
+    for e in range(n_z - 1, 1, -1):
         for i in order_i:
             for to, ok in ((z + e, z + e < n_z), (z - e, z >= e)):
                 @pl.when(ok)
@@ -253,6 +262,25 @@
                     def _():
                         unit(s, r)
                         unit(r, s)
+
+    def w_group(g):
+        for i in order_i:
+            for s, ok, _ in sides(g):
+                @pl.when(ok)
+                def _(i=i, s=s):
+                    w_in(i, s)
+
+    def w_pass(g):
+        for q in range(n_z - g, 0, -1):
+            for i in order_i:
+                for k, (s, ok, step) in enumerate(sides(g)):
+                    e = jnp.where(z // (n_z // 2) == k, q, q - 1)
+                    to = z + step * e
+
+                    @pl.when(ok & (e > 0) & (to >= 0) & (to < n_z))
+                    def _(i=i, s=s, to=to):
+                        w_wait(i, s, to)
+                        w_hop(i, s, to, fwd.at[i, s, to])
 
     for g in range(1, n_z):
         for arr in range(2):
@@ -267,20 +295,13 @@
             unit(z, z)
         else:
             finish(g - 1)
-        for i in order_i:
-            for s, ok, _ in sides(g):
-                @pl.when(ok)
-                def _(i=i, s=s):
-                    w_in(i, s)
-        for e in range(1, n_z - g):
-            for i in order_i:
-                for s, ok, step in sides(g):
-                    to = z + step * e
-
-                    @pl.when(ok & (to >= 0) & (to < n_z))
-                    def _(i=i, s=s, to=to):
-                        w_wait(i, s, to)
-                        w_hop(i, s, to, fwd.at[i, s, to])
+        if g == 1:
+            w_group(g)
+            w_pass(g)
+        else:
+            w_pass(g)
+            w_group(g)
+
     for arr in range(2):
         y_tok_wait(arr, last)
 
@@ -305,11 +326,11 @@
     x_in(2, last)
     x_in(0, last)
     whole(2)
+    whole(0)
     x_in(1, last)
-    whole(0)
     whole(1)
 
-    n_cut = 4
+    n_cut = 2
     cut = width // n_cut
 
     def yi_copy(p, n):
@@ -426,6 +447,13 @@
         dx_copy(p).start()
         acc[here, mine] = acc[here, mine] + dn_in[p, here].astype(F32)
 
+    def down_out(p):
+        rows = ds(p, hid)
+        return pltpu.make_async_copy(down_ref.at[rows], down_hbm.at[rows], out_sem.at[p])
+
+    def grad_out(i, rows):
+        return pltpu.make_async_copy(grad_ref.at[rows], grad_hbm.at[0, rows], out_sem.at[n_z + i])
+
     def dx_add(p):
         dx_copy(p).wait_recv()
         total = acc[ds(fx, hid), ds(p * 2 + c, cols)] + dx_in[p].astype(F32)
@@ -433,6 +461,7 @@
         @pl.when(p == z)
         def _():
             down_ref[ds(z, hid)] = total
+            down_out(z).start()
 
         @pl.when(p != z)
         def _():
@@ -447,7 +476,7 @@
 
     for k in range(2, n_z - 1):
         y_add(far(k))
-    for k in range(n_z - 1):
+    for k in range(n_z - 2):
         dx_add(far(k))
 
     own_rows = ds(fx * 2 + fy, quarter)
@@ -456,7 +485,7 @@
     d_rows = ds((1 - fx) * 2 + 1 - fy, quarter)
 
     def ag_copy(i, n, rows, dev):
-        src = grad_ref.at[0, rows, ds(n, cut)]
+        src = grad_ref.at[rows, ds(n, cut)]
         return rc(src, src, ag_ss.at[i, n], ag_rs.at[i, n], dev)
 
     below = (z > 0) & ((z - 1) // (n_z // 2) == top)
@@ -475,26 +504,34 @@
         gain(n_z + 1)
         pl.when(below)(lambda: gain(z))
         pl.when(above)(lambda: gain(n_z))
-        grad_ref[0, own_rows, at] = total[...].astype(BF16)
+        grad_ref[own_rows, at] = total[...].astype(BF16)
         ag_copy(1, n, own_rows, dev_y).start()
         ag_copy(0, n, own_rows, dev_x).start()
 
-    dx_add(z)
+    dx_add(far(n_z - 2))
 
     @pl.loop(0, n_cut)
     def _(n):
         ag_copy(1, n, y_rows, dev_y).wait_recv()
         ag_copy(2, n, y_rows, dev_x).start()
+
+    dx_add(z)
 
     for j in range(1, n_z):
         s = near(j)
         dst = dz_in.at[s]
         rc(dst, dst, dz_ss.at[s], dz_rs.at[s], partner).wait_recv()
         down_ref[ds(s, hid)] = dz_in[s].astype(F32)
-
+        down_out(s).start()
+
+    grad_out(0, own_rows).start()
+    grad_out(1, y_rows).start()
     for n in range(n_cut):
         ag_copy(0, n, x_rows, dev_x).wait_recv()
+    grad_out(2, x_rows).start()
+    for n in range(n_cut):
         ag_copy(2, n, d_rows, dev_x).wait_recv()
+    grad_out(3, d_rows).start()
 
     for arr in range(2):
         for p in range(n_z):
@@ -541,6 +578,10 @@
         ag_copy(0, n, own_rows, dev_x).wait_send()
         ag_copy(1, n, own_rows, dev_y).wait_send()
         ag_copy(2, n, y_rows, dev_x).wait_send()
+    for p in range(n_z):
+        down_out(p).wait()
+    for i, rows in enumerate((own_rows, y_rows, x_rows, d_rows)):
+        grad_out(i, rows).wait()
 
 
 def spread(n_tp, inputs, cotangent, gate_weight, up_weight, down_weight):
@@ -549,7 +590,6 @@
     n_z = n_tp // 2
     hid, cols, half, quarter = hid_all // n_z, width // n_tp, n_tok // 2, n_tok // 4
     dma = pltpu.SemaphoreType.DMA
-    vmem = pl.BlockSpec(memory_space=pltpu.VMEM)
     anyspace = pl.BlockSpec(memory_space=pl.ANY)
     return pl.pallas_call(
         functools.partial(kernel, n_tp),
@@ -558,9 +598,14 @@
             jax.ShapeDtypeStruct((1, n_tok, width), BF16),
             jax.ShapeDtypeStruct((hid_all, cols), F32),
         ),
-        in_specs=[anyspace, anyspace, vmem, vmem, vmem],
-        out_specs=(vmem, vmem),
+        in_specs=[anyspace] * 5,
+        out_specs=(anyspace, anyspace),
         scratch_shapes=[
+            pltpu.VMEM(gate_weight.shape, BF16),
+            pltpu.VMEM(up_weight.shape, BF16),
+            pltpu.VMEM(down_weight.shape, BF16),
+            pltpu.VMEM((n_tok, width), BF16),
+            pltpu.VMEM((hid_all, cols), F32),
             pltpu.VMEM((2, n_z * half, width), BF16),
             pltpu.VMEM((3, n_tp, 2 * hid, cols), BF16),
             pltpu.VMEM((hid_all, cols), BF16),
@@ -573,7 +618,7 @@
             pltpu.VMEM((half, 2 * hid), BF16),
             pltpu.VMEM((half, 2 * hid), BF16),
             pltpu.VMEM((half, 2 * hid), BF16),
-            pltpu.VMEM((quarter, width // 4), F32),
+            pltpu.VMEM((quarter, width // 2), F32),
             pltpu.VMEM((n_z, 2 * hid, cols), BF16),
             pltpu.VMEM((n_z, 2 * hid, cols), BF16),
             pltpu.VMEM((n_z, hid, cols), BF16),
@@ -581,10 +626,10 @@
             pltpu.VMEM((n_z, hid, cols), BF16),
             pltpu.VMEM((n_z, hid, cols), BF16),
             pltpu.VMEM((3, n_z, n_z, hid, cols), BF16),
-            dma((2,)), dma((2, n_z, 2)), dma((2, n_z)), dma((2, n_z)), dma((2, n_z)),
+            dma((5,)), dma((n_z + 4,)), dma((2, n_z, 2)), dma((2, n_z)), dma((2, n_z)), dma((2, n_z)),
             dma((3, n_z, n_z)), dma((3, n_z, n_z)), dma((3, n_z)), dma((3, n_z)),
             dma((3, 2, n_z)), dma((3, 2, n_z)),
-            dma((n_z, 4)), dma((n_z, 4)), dma((n_z, 4)), dma((n_z + 2, 4)), dma((3, 4)), dma((3, 4)),
+            dma((n_z, 2)), dma((n_z, 2)), dma((n_z, 2)), dma((n_z + 2, 2)), dma((3, 2)), dma((3, 2)),
             dma((n_z,)), dma((n_z,)), dma((n_z,)), dma((n_z,)), dma((n_z,)), dma((n_z,)),
         ],
         compiler_params=pltpu.CompilerParams(
@@ -602,8 +647,8 @@
         n_z = n_tp // 2
         fits = (
             n_fs == 4
-            and n_tp % 2 == 0
-            and hid_all % (n_z * 16) == 0
+            and n_tp == 2 * n_z
+            and hid_all % (n_z * 32) == 0
             and width % (n_tp * 128) == 0
             and n_tok % 64 == 0
             and (3 * n_tok + 9 * hid_all) * n_z * width + 18 * hid_all * width < 62_000_000 * n_z

time: 151 us -> 146 us (0.967)
  Pallas kernels: 146 us -> 142 us
    pallas_call x1, Pallas kernels: 146 us -> 142 us  [spread(): pl.pallas_call(functools.partial(kernel, n_tp), name='spread_hidden', out...]
where the time goes in v4:
time: 146 us
  Pallas kernels  142 us (97%)
  local copies, waits for them, and re-layouts  3.73 us (3%)
    pallas_call x1, Pallas kernels, spread(): pl.pallas_call(functools.partial(kernel, n_tp), name='spread_hidden', out...  142 us
    unnamed x4, local copies, waits for them, and re-layouts  3.73 us

profile of v4, /device:TPU:0, one launch (start us, length us, event | category | flops | bytes accessed | tf_op | source)
XLA Modules:
  0.0 146.2 jit_solution(5485306858138904945)
XLA Ops:
  0.6 141.8 %spread_hidden.1 = (bf16[1,320,2048]{2,1,0:T(8,128)(2,1)}, f32[1408,256]{1,0:T(8,128)}) custom-call(bf16[1,320,2048]{2,1,0:T(8,128)(2,1)} %x_ref.1, bf16[1,320,2048]{2,1,0:T(8,128)(2,1)} %ct_ref.1, bf16[256,1408]{1,0:T(8,128)(2,1)} %wg_hbm.1, bf16[256,1408]{1,0:T(8,128)(2,1)} %wu_hbm.1, bf16[1408,256]{1,0:T(8,128)(2,1)} %wd_hbm.1), custom_call_target="tpu_custom_call" | custom-call | tf_op jit(solution)/shard_map/spread_hidden/pallas_call | solution.py:594
  142.4 0.0 copy-start
  142.4 2.6 %copy.9 = bf16[1,320,2048]{2,1,0:T(8,128)(2,1)} copy(bf16[1,320,2048]{2,1,0:T(8,128)(2,1)} %get-tuple-element.4) | data formatting | bytes 2621440
  145.1 0.0 copy-done
  145.1 1.1 copy.10
Async XLA Ops:
  142.4 2.6 %copy-start = (f32[1408,256]{1,0:T(8,128)S(1)}, f32[1408,256]{1,0:T(8,128)}, u32[]{:S(2)}) copy-start(f32[1408,256]{1,0:T(8,128)} %get-tuple-element.5) | copy-start | bytes 4325380

commit v5 on v4

--- a/solution.py
+++ b/solution.py
@@ -311,24 +311,24 @@
         def _():
             unit(last, r)
 
+    def part_pre(i, m):
+        rows = ds(m, 2 * half)
+        total = pre[i, rows]
+        for k in range(2):
+            at = ds(last * 2 + k, cols)
+            total += contract_hidden(tok[1 if i == 2 else 0, rows, at], wts[i, last * 2 + k])
+        pre[i, rows] = total
+
     def whole(i):
         arrived(i, last)
-
-        @pl.loop(0, n_z // 2)
-        def _(m):
-            rows = ds(m, 2 * half)
-            total = pre[i, rows]
-            for k in range(2):
-                at = ds(last * 2 + k, cols)
-                total += contract_hidden(tok[1 if i == 2 else 0, rows, at], wts[i, last * 2 + k])
-            pre[i, rows] = total
+        pl.loop(0, n_z // 2)(lambda m: part_pre(i, m))
 
     x_in(2, last)
     x_in(0, last)
     whole(2)
     whole(0)
     x_in(1, last)
-    whole(1)
+    arrived(1, last)
 
     n_cut = 2
     cut = width // n_cut
@@ -413,9 +413,18 @@
 
     outer = (z == 0) | (z == n_z - 1)
 
+    first = far(0) // 2
+    part_pre(1, first)
+
     @pl.loop(0, n_z)
     def _(j):
         sweep(far(j))
+
+        @pl.when(j == 0)
+        def _():
+            @pl.loop(1, n_z // 2)
+            def _(m):
+                part_pre(1, (first + m) % (n_z // 2))
 
         @pl.when((j == n_z - 2) & outer)
         def _():

time: 146 us -> 146 us (level)
  no operation moved by 1% of the time
where the time goes in v5:
time: 146 us
  Pallas kernels  141 us (97%)
  local copies, waits for them, and re-layouts  3.73 us (3%)
    pallas_call x1, Pallas kernels, spread(): pl.pallas_call(functools.partial(kernel, n_tp), name='spread_hidden', out...  141 us
    unnamed x4, local copies, waits for them, and re-layouts  3.73 us

profile of v5, /device:TPU:0, one launch (start us, length us, event | category | flops | bytes accessed | tf_op | source)
XLA Modules:
  0.0 145.7 jit_solution(5451866282174502802)
XLA Ops:
  0.6 141.3 %spread_hidden.1 = (bf16[1,320,2048]{2,1,0:T(8,128)(2,1)}, f32[1408,256]{1,0:T(8,128)}) custom-call(bf16[1,320,2048]{2,1,0:T(8,128)(2,1)} %x_ref.1, bf16[1,320,2048]{2,1,0:T(8,128)(2,1)} %ct_ref.1, bf16[256,1408]{1,0:T(8,128)(2,1)} %wg_hbm.1, bf16[256,1408]{1,0:T(8,128)(2,1)} %wu_hbm.1, bf16[1408,256]{1,0:T(8,128)(2,1)} %wd_hbm.1), custom_call_target="tpu_custom_call" | custom-call | tf_op jit(solution)/shard_map/spread_hidden/pallas_call | solution.py:603
  142.0 0.0 copy-start
  142.0 2.6 %copy.9 = bf16[1,320,2048]{2,1,0:T(8,128)(2,1)} copy(bf16[1,320,2048]{2,1,0:T(8,128)(2,1)} %get-tuple-element.4) | data formatting | bytes 2621440
  144.6 0.0 copy-done
  144.6 1.1 copy.10
Async XLA Ops:
  142.0 2.6 %copy-start = (f32[1408,256]{1,0:T(8,128)S(1)}, f32[1408,256]{1,0:T(8,128)}, u32[]{:S(2)}) copy-start(f32[1408,256]{1,0:T(8,128)} %get-tuple-element.5) | copy-start | bytes 4325380
